TPU v7x, 128 devices: a whole 4x4x4 slice. The times are simulated.
128 devices in a mesh: sp: 16 (over z, x), fs: 4 (over y), tp: 2 (over core).
Axes of the slice: x: 4, y: 4, z: 4, core: 2. Of those that a mesh axis runs over, the one named last changes fastest.
Arguments:
- tokens: bfloat16 [4, 8192, 2048], P('fs', 'sp', 'tp'), may hold values from -6 to 6
- norm_gain: float32 [2048], replicated, may hold values from 0.1 to 1.9
- w_pool_in: bfloat16 [2048, 512], P('fs', 'tp'), may hold values from -0.125 to 0.125
- w_query: bfloat16 [2048, 1024], P('fs', 'tp'), may hold values from -0.125 to 0.125
- w_key: bfloat16 [2048, 1024], P('fs', 'tp'), may hold values from -0.125 to 0.125
- w_value: bfloat16 [2048, 1024], P('fs', 'tp'), may hold values from -0.125 to 0.125
- query_gain: float32 [64], replicated, may hold values from 1.5 to 2.5
- key_gain: float32 [64], replicated, may hold values from 1.5 to 2.5
- stick_offset: float32 [16], P('tp'), as said below
- pool_mix: bfloat16 [4, 128, 128], P('tp'), may hold values from -0.5 to 0.5
- pool_scale: float32 [512], P('tp'), may hold values from 0.2 to 4, as said below
- pool_gain: bfloat16 [512], P('tp'), may hold values from 0.099609375 to 1.8984375
- attn_gain: bfloat16 [1024], P('tp'), may hold values from 0.099609375 to 1.8984375
- w_out_pool: bfloat16 [512, 2048], P('tp', 'fs'), may hold values from -0.15625 to 0.15625
- w_out_attn: bfloat16 [1024, 2048], P('tp', 'fs'), may hold values from -0.15625 to 0.15625
Outputs:
- mixed: bfloat16 [4, 8192, 2048], P('fs', ('sp', 'tp'))
Inputs may be any that keep to these rules, and one draw needn't show every extreme that they name: `stick_offset`: per head, negative. `pool_scale`: positive channel scales.
All inputs are finite; a program needn't handle non-finite values.
Results may differ from a plain program's by a relative error of at most 0.013.
Values may be sent and summed in bfloat16 or wider, within the bound.
A program may use at most 192 MiB of HBM per device.

v0:
```python
import math
import jax
import jax.numpy as jnp
from jax import lax
from jax.sharding import PartitionSpec as P

HEADS = 16
HEAD_DIM = 64
POOL = 512
POOL_GROUPS = 4
EPS = 1e-06


def sent_to_all(shard, axis):
    devices = lax.axis_size(axis)
    return lax.all_to_all(
        jnp.broadcast_to(shard[None], (devices, *shard.shape)), axis, 0, 0, tiled=True
    )


def in_order(parts, dim):
    lengths = list(parts.shape[1:])
    lengths[dim] *= parts.shape[0]
    return jnp.moveaxis(parts, 0, dim).reshape(lengths)


def gathered_copies(shard, axis, dim):
    parts = sent_to_all(shard, axis)
    return in_order(parts, dim)


def in_one_piece(arrays, axis, dim, along):
    both = jnp.concatenate(arrays, axis=along)
    whole, at, outs = (lax.all_gather(both, axis, axis=dim, tiled=True), 0, [])
    for a in arrays:
        outs.append(lax.slice_in_dim(whole, at, at + a.shape[along], axis=along))
        at += a.shape[along]
    return tuple(outs)


def shifted_2(value, axis, steps):
    count = lax.axis_size(axis)
    initial, last = (max(0, -steps), min(count, count - steps))
    return lax.ppermute(value, axis, [(source, source + steps) for source in range(initial, last)])


def partner_2(shard, axis, distance):
    return lax.ppermute(shard, axis, [(i, i ^ 1 << distance) for i in range(lax.axis_size(axis))])


def head_norm(projected, gain, head_count):
    split = projected.reshape(projected.shape[0], head_count, HEAD_DIM)
    factor = lax.rsqrt(jnp.mean(split * split, axis=-1, keepdims=True) + EPS)
    return (split * factor * gain).astype(jnp.bfloat16)


def stick_block(query, key_heads, value_heads, offset, carried, row_offset, score_scale):
    scores = (
        jnp.einsum("thd,khd->htk", query, key_heads, preferred_element_type=jnp.float32)
        * score_scale
        + offset[:, None, None]
    )
    keep = jax.nn.log_sigmoid(-scores)
    if row_offset is not None:
        shape = (query.shape[0], key_heads.shape[0])
        earlier = (
            lax.broadcasted_iota(jnp.int32, shape, 1)
            < lax.broadcasted_iota(jnp.int32, shape, 0) + row_offset
        )
        keep = jnp.where(earlier[None], keep, 0.0)
    running = jnp.cumsum(keep, axis=2)
    block_total = running[:, :, -1]
    log_weight = (
        jax.nn.log_sigmoid(scores) + block_total[:, :, None] - running + carried[:, :, None]
    )
    weight = jnp.exp(log_weight)
    if row_offset is not None:
        weight = jnp.where(earlier[None], weight, 0.0)
    weight = weight.astype(jnp.bfloat16)
    block_out = jnp.einsum("htk,khd->thd", weight, value_heads, preferred_element_type=jnp.float32)
    return (block_out, block_total)


def branch_norm(values_in, squares, width, gain):
    values_f = values_in.astype(jnp.float32)
    factor = lax.rsqrt(squares / width + EPS)
    return (values_f * factor[:, None] * gain.astype(jnp.float32)).astype(jnp.bfloat16)


def shards(
    tokens,
    norm_gain,
    w_pool_in,
    w_query,
    w_key,
    w_value,
    query_gain,
    key_gain,
    stick_offset,
    pool_mix,
    pool_scale,
    pool_gain,
    attn_gain,
    w_out_pool,
    w_out_attn,
):
    whole = gathered_copies(tokens, "tp", 2)[0]
    whole_f = whole.astype(jnp.float32)
    normed = (
        whole_f * lax.rsqrt(jnp.mean(whole_f * whole_f, axis=-1, keepdims=True) + EPS) * norm_gain
    ).astype(jnp.bfloat16)
    row_count = normed.shape[0]
    pieces = in_one_piece((w_pool_in, w_query, w_key, w_value), "fs", 0, 1)
    pool_raw, query_raw, key_raw, value_raw = tuple(
        (jnp.dot(normed, piece, preferred_element_type=jnp.float32) for piece in pieces)
    )
    head_count = query_raw.shape[1] // HEAD_DIM
    query = head_norm(query_raw, query_gain, head_count)
    key_heads = head_norm(key_raw, key_gain, head_count)
    value_heads = value_raw.astype(jnp.bfloat16).reshape(row_count, head_count, HEAD_DIM)
    reach = 16
    pool_in = pool_raw.astype(jnp.bfloat16)
    previous = shifted_2(pool_in[row_count - reach :], "sp", 1)
    extended = jnp.concatenate([previous, pool_in], axis=0).astype(jnp.float32)
    pool_cols = pool_in.shape[1]
    group_ch = POOL // POOL_GROUPS
    local_groups = pool_cols // group_ch
    group_ids = (
        lax.axis_index("tp") * local_groups + jnp.arange(pool_cols, dtype=jnp.int32) // group_ch
    )
    window = jnp.left_shift(jnp.int32(2), group_ids)
    summed = jnp.zeros((row_count, pool_cols), jnp.float32)
    for behind in range(reach):
        shifted = extended[reach - behind : reach - behind + row_count]
        summed = summed + jnp.where(behind < window[None, :], shifted, 0.0)
    sp_index = lax.axis_index("sp")
    position = sp_index * row_count + jnp.arange(row_count, dtype=jnp.int32)
    counted = jnp.minimum(position[:, None] + 1, window[None, :]).astype(jnp.float32)
    centered = (summed / counted - extended[reach:]).astype(jnp.bfloat16)
    pooled = jnp.einsum(
        "tgc,gcd->tgd",
        centered.reshape(row_count, local_groups, group_ch),
        pool_mix,
        preferred_element_type=jnp.float32,
    )
    pool_out = (pooled.reshape(row_count, pool_cols) * pool_scale).astype(jnp.bfloat16)
    score_scale = 1.0 / math.sqrt(HEAD_DIM)
    sp_count = lax.axis_size("sp")
    key_value = jnp.stack([key_heads, value_heads])
    everything = lax.all_gather(key_value, "sp", axis=1, tiled=True)
    half = row_count // 2
    bit_count = sp_count.bit_length() - 1

    def run_rows(query_rows, source, row_offset):
        start_carry = jnp.zeros((head_count, query_rows.shape[0]), jnp.float32)
        diagonal = lax.dynamic_slice_in_dim(everything, source * row_count, row_count, 1)
        first_out, first_carry = stick_block(
            query_rows, diagonal[0], diagonal[1], stick_offset, start_carry, row_offset, score_scale
        )

        def turn(turn_index, state):
            acc_out, acc_carry = state
            block = lax.dynamic_slice_in_dim(
                everything, (source - turn_index) * row_count, row_count, 1
            )
            block_out, block_total = stick_block(
                query_rows, block[0], block[1], stick_offset, acc_carry, None, score_scale
            )
            return (acc_out + block_out, acc_carry + block_total)

        result, unused = lax.fori_loop(1, source + 1, turn, (first_out, first_carry))
        return result.reshape(query_rows.shape[0], head_count * HEAD_DIM).astype(jnp.bfloat16)

    guest_query = query[half:]
    for bit in range(bit_count):
        guest_query = partner_2(guest_query, "sp", bit)
    partner = sp_count - 1 - sp_index
    own_rows = run_rows(query[:half], sp_index, 0)
    guest_rows = run_rows(guest_query, partner, half)
    for bit in range(bit_count):
        guest_rows = partner_2(guest_rows, "sp", bit)
    attn_out = jnp.concatenate([own_rows, guest_rows], axis=0)
    w_pool_cols, w_attn_cols = (
        lax.all_gather(w_out_pool, "fs", axis=1, tiled=True),
        lax.all_gather(w_out_attn, "fs", axis=1, tiled=True),
    )
    pool_rows, attn_rows = (
        lax.all_to_all(pool_out, "tp", split_axis=0, concat_axis=1, tiled=True),
        lax.all_to_all(attn_out, "tp", split_axis=0, concat_axis=1, tiled=True),
    )
    w_pool_all, w_attn_all, pool_gain_all, attn_gain_all = (
        lax.all_gather(w_pool_cols, "tp", axis=0, tiled=True),
        lax.all_gather(w_attn_cols, "tp", axis=0, tiled=True),
        lax.all_gather(pool_gain, "tp", axis=0, tiled=True),
        lax.all_gather(attn_gain, "tp", axis=0, tiled=True),
    )
    pool_f = pool_rows.astype(jnp.float32)
    attn_f = attn_rows.astype(jnp.float32)
    pool_normed = branch_norm(pool_rows, jnp.sum(pool_f * pool_f, axis=-1), POOL, pool_gain_all)
    attn_normed = branch_norm(
        attn_rows, jnp.sum(attn_f * attn_f, axis=-1), HEADS * HEAD_DIM, attn_gain_all
    )
    mixed = jnp.dot(pool_normed, w_pool_all, preferred_element_type=jnp.float32) + jnp.dot(
        attn_normed, w_attn_all, preferred_element_type=jnp.float32
    )
    return mixed.astype(jnp.bfloat16)[None]


def solution(mesh):
    in_specs = (
        P("fs", "sp", "tp"),
        P(),
        P("fs", "tp"),
        P("fs", "tp"),
        P("fs", "tp"),
        P("fs", "tp"),
        P(),
        P(),
        P("tp"),
        P("tp", None, None),
        P("tp"),
        P("tp"),
        P("tp"),
        P("tp", "fs"),
        P("tp", "fs"),
    )
    out_specs = P("fs", ("sp", "tp"), None)
    return jax.shard_map(shards, mesh=mesh, in_specs=in_specs, out_specs=out_specs, check_vma=False)
```

profile of v0, /device:TPU:103, one launch (start us, length us, event | category | flops | bytes accessed | tf_op | source)
XLA Modules:
  0.0 761.2 jit_solution(1497514801564157925)
XLA Ops:
  11.9 5.5 all-to-all-start
  27.3 57.7 %all-gather.9.cloned.1.call-done = bf16[2048,1792]{1,0:T(8,128)(2,1)} async-done(((bf16[512,1792]{1,0:T(8,128)(2,1)}), bf16[2048,1792]{1,0:T(8,128)(2,1)}) %all-gather.9.cloned.1.call-update) | async-done | bytes 7340048 | tf_op jit(solution)/shard_map/all_gather | solution.py:34
  101.0 17.3 %all-gather.17.cloned.1.call-done = bf16[512,2048]{1,0:T(8,128)(2,1)} async-done(((bf16[512,512]{1,0:T(8,128)(2,1)}), bf16[512,2048]{1,0:T(8,128)(2,1)}) %all-gather.17.cloned.1.call-update) | async-done | bytes 2097168 | tf_op jit(solution)/shard_map/all_gather | solution.py:185
  134.2 8.0 %all-gather.11.cloned.1.call-done = bf16[256,2048]{1,0:T(8,128)(2,1)} async-done(((bf16[256,512]{1,0:T(8,128)(2,1)}), bf16[256,2048]{1,0:T(8,128)(2,1)}) %all-gather.11.cloned.1.call-update) | async-done | bytes 1048592 | tf_op jit(solution)/shard_map/all_gather | solution.py:184
  146.6 6.6 all-to-all-start.1
  154.5 8.8 %collective-permute-done.3 = bf16[256,8,64]{0,2,1:T(8,128)(2,1)S(1)} collective-permute-done((bf16[256,8,64]{0,2,1:T(8,128)(2,1)S(1)}, bf16[256,8,64]{0,2,1:T(8,128)(2,1)S(1)}, u32[]{:S(2)}, u32[]{:S(2)}) %collective-permute-start.3) | collective-permute-done | bytes 262176 | tf_op jit(solution)/shard_map/ppermute | solution.py:48
  165.4 5.4 collective-permute-done.4
  170.8 97.9 %all-gather.15.cloned.1.call-done = bf16[2,8192,8,64]{1,3,2,0:T(8,128)(2,1)} async-done(((bf16[2,512,8,64]{1,3,2,0:T(8,128)(2,1)}), bf16[2,8192,8,64]{1,3,2,0:T(8,128)(2,1)}) %all-gather.15.cloned.1.call-update) | async-done | bytes 16777232 | tf_op jit(solution)/shard_map/all_gather | solution.py:150
  270.6 10.6 %fusion.63 = (f32[8,256,512]{2,1,0:T(8,128)}, f32[8,256,512]{2,1,0:T(8,128)}, f32[8,256,512]{2,1,0:T(8,128)}) fusion(f32[8]{0:T(128)S(1)} %copy-done.14, pred[256,512]{1,0:T(8,128)(4,1)S(1)} %get-tuple-element.157, f32[8,256,512]{2,1,0:T(8,128)S(1)} %fusion.97, pred[256,512]{1,0:T(8,128)(4,1)S(1)} %get-tuple-element.156, ...), kind=kOutput, calls=%fused_computation.79 | convolution fusion | flops 155189248 | bytes 17826308 | tf_op jit(solution)/shard_map/thd,khd->htk/dot_general | solution.py:59
  281.2 5.7 copy.122
  286.9 5.6 copy.124
  297.5 5.3 copy.125
  304.8 6.4 fusion.88
  311.4 14.4 %collective-permute-start.5 = (bf16[256,512]{0,1:T(8,128)(2,1)S(1)}, bf16[256,512]{0,1:T(8,128)(2,1)S(1)}, u32[]{:S(2)}, u32[]{:S(2)}) collective-permute-start(bf16[256,512]{0,1:T(8,128)(2,1)S(1)} %bitcast.254), channel_id=1, source_target_pairs={{0,8},{8,0},{16,24},{24,16},{32,40},{40,32},{48,56},{56,48},{64,72... | collective-permute-start | bytes 786440 | tf_op jit(solution)/shard_map/ppermute | solution.py:48
  330.5 28.5 %collective-permute-start.6 = (bf16[256,512]{0,1:T(8,128)(2,1)S(1)}, bf16[256,512]{0,1:T(8,128)(2,1)S(1)}, u32[]{:S(2)}, u32[]{:S(2)}) collective-permute-start(bf16[256,512]{0,1:T(8,128)(2,1)S(1)} %collective-permute-done.5), channel_id=1, source_target_pairs={{0,16},{8,24},{16,0},{24,8},{32,48},{40,56},{48,32},{56,40},{64,80... | collective-permute-start | bytes 786440 | tf_op jit(solution)/shard_map/ppermute | solution.py:48
  361.2 5.3 copy.123
  368.3 53.3 %collective-permute-start.7 = (bf16[256,512]{0,1:T(8,128)(2,1)S(1)}, bf16[256,512]{0,1:T(8,128)(2,1)S(1)}, u32[]{:S(2)}, u32[]{:S(2)}) collective-permute-start(bf16[256,512]{0,1:T(8,128)(2,1)S(1)} %collective-permute-done.6), channel_id=1, source_target_pairs={{0,32},{8,40},{16,48},{24,56},{32,0},{40,8},{48,16},{56,24},{64,96... | collective-permute-start | bytes 786440 | tf_op jit(solution)/shard_map/ppermute | solution.py:48
  421.7 6.4 fusion.85
  428.1 110.3 %collective-permute-start.8 = (bf16[256,512]{0,1:T(8,128)(2,1)S(1)}, bf16[256,512]{0,1:T(8,128)(2,1)S(1)}, u32[]{:S(2)}, u32[]{:S(2)}) collective-permute-start(bf16[256,512]{0,1:T(8,128)(2,1)S(1)} %collective-permute-done.7), channel_id=1, source_target_pairs={{0,64},{8,72},{16,80},{24,88},{32,96},{40,104},{48,112},{56,120},{... | collective-permute-start | bytes 786440 | tf_op jit(solution)/shard_map/ppermute | solution.py:48
  538.4 200.5 %while.24 = (s32[]{:T(128)}, f32[256,8,64]{0,2,1:T(8,128)S(1)}, f32[8,256]{1,0:T(8,128)S(1)}, s32[]{:T(128)}, s32[]{:T(128)}, /*index=5*/bf16[2,8192,8,64]{1,3,2...) while((s32[]{:T(128)}, f32[256,8,64]{0,2,1:T(8,128)S(1)}, ...), condition=%wide.region_9.10_spmd, body=%wide.region_6.9_spmd.sunk | while | flops 426934272 | bytes 44548372 | solution.py:171
  547.0 4.7 fusion.179
  560.4 4.7 fusion.179
  573.7 4.7 fusion.179
  587.1 4.7 fusion.179
  600.5 4.7 fusion.179
  613.8 4.7 fusion.179
  627.2 4.7 fusion.179
  653.9 4.7 fusion.179
  667.3 4.7 fusion.179
  694.1 4.7 fusion.179
  720.8 4.7 fusion.179
  739.3 6.9 all_to_all.28
  (270 shorter events, 227.0 us)
Async XLA Ops:
  6.5 137.0 %copy-start = (bf16[2,128,128]{2,1,0:T(8,128)(2,1)S(1)}, bf16[2,128,128]{2,1,0:T(8,128)(2,1)}, u32[]{:S(2)}) copy-start(bf16[2,128,128]{2,1,0:T(8,128)(2,1)} %param.28) | copy-start | bytes 196612
  6.5 3.7 copy-start.5
  6.5 78.5 %all-gather.9.cloned.1.call-start = ((), (), s32[]{:S(2)}) async-start(), calls=%async_computation.3 | async-start | bytes 9175040 | tf_op jit(solution)/shard_map/all_gather | solution.py:34
  9.5 8.7 %copy-start.7 = (f32[2048]{0:T(1024)S(1)}, f32[2048]{0:T(1024)}, u32[]{:S(2)}) copy-start(f32[2048]{0:T(1024)} %param.20) | copy-start | bytes 24580
  9.5 108.8 %all-gather.17.cloned.1.call-start = ((), (), s32[]{:S(2)}) async-start(), calls=%async_computation.7 | async-start | bytes 2621440 | tf_op jit(solution)/shard_map/all_gather | solution.py:185
  11.9 8.1 %all-to-all-start = ((bf16[2,1,512,1024]{3,2,1,0:T(8,128)(2,1)}), bf16[2,1,512,1024]{3,2,1,0:T(8,128)(2,1)}, u32[]{:S(2)}, u32[]{:S(2)}) async-start(bf16[2,1,512,1024]{3,2,1,0:T(8,128)(2,1)} %broadcast_in_dim.182), calls=%async_computation | async-start | bytes 4194304 | tf_op jit(solution)/shard_map/all_to_all | solution.py:16
  17.4 124.8 %all-gather.11.cloned.1.call-start = ((), (), s32[]{:S(2)}) async-start(), calls=%async_computation.4 | async-start | bytes 1310720 | tf_op jit(solution)/shard_map/all_gather | solution.py:184
  18.1 250.7 %all-gather.15.cloned.1.call-start = ((), (), s32[]{:S(2)}) async-start(), calls=%async_computation.6 | async-start | bytes 17825792 | tf_op jit(solution)/shard_map/all_gather | solution.py:150
  92.9 3.7 copy-start.11
  92.9 3.9 copy-start.3
  100.9 646.2 %all-gather.19.cloned.1.call-start = ((), (), s32[]{:S(2)}) async-start(), calls=%async_computation.8 | async-start | bytes 6291456 | tf_op jit(solution)/shard_map/all_gather | solution.py:193
  118.3 632.3 %all-gather.13.cloned.1.call-start = ((), (), s32[]{:S(2)}) async-start(), calls=%async_computation.5 | async-start | bytes 3145728 | tf_op jit(solution)/shard_map/all_gather | solution.py:192
  121.2 3.7 copy-start.12
  121.2 4.6 copy-start.4
  124.9 4.3 copy-start.13
  124.9 6.9 copy-start.10
  125.2 17.1 %collective-permute-start.1 = (bf16[256,8,64]{0,2,1:T(8,128)(2,1)S(1)}, bf16[256,8,64]{0,2,1:T(8,128)(2,1)S(1)}, u32[]{:S(2)}, u32[]{:S(2)}) collective-permute-start(bf16[256,8,64]{0,2,1:T(8,128)(2,1)S(1)} %get-tuple-element.132), channel_id=1, source_target_pairs={{0,8},{8,0},{16,24},{24,16},{32,40},{40,32},{48,56},{56,48},{64,72... | collective-permute-start | bytes 786440 | tf_op jit(solution)/shard_map/ppermute | solution.py:48
  127.9 14.4 %collective-permute-start = (bf16[16,256]{1,0:T(8,128)(2,1)S(1)}, bf16[16,256]{1,0:T(8,128)(2,1)S(1)}, u32[]{:S(2)}, u32[]{:S(2)}) collective-permute-start(bf16[16,256]{1,0:T(8,128)(2,1)S(1)} %slice.170), channel_id=1, source_target_pairs={{0,8},{8,16},{16,24},{24,32},{32,40},{40,48},{48,56},{56,64},{64,7... | collective-permute-start | bytes 24584 | tf_op jit(solution)/shard_map/ppermute | solution.py:44
  142.3 10.9 %collective-permute-start.2 = (bf16[256,8,64]{0,2,1:T(8,128)(2,1)S(1)}, bf16[256,8,64]{0,2,1:T(8,128)(2,1)S(1)}, u32[]{:S(2)}, u32[]{:S(2)}) collective-permute-start(bf16[256,8,64]{0,2,1:T(8,128)(2,1)S(1)} %collective-permute-done.1), channel_id=1, source_target_pairs={{0,16},{8,24},{16,0},{24,8},{32,48},{40,56},{48,32},{56,40},{64,80... | collective-permute-start | bytes 786440 | tf_op jit(solution)/shard_map/ppermute | solution.py:48
  143.6 2.3 copy-start.9
  146.6 124.0 %copy-start.14 = (f32[8]{0:T(128)S(1)}, f32[8]{0:T(128)}, u32[]{:S(2)}) copy-start(f32[8]{0:T(128)} %param.27) | copy-start | bytes 100
  146.6 7.8 %all-to-all-start.1 = ((bf16[2,256,256]{2,1,0:T(8,128)(2,1)}), bf16[2,256,256]{2,1,0:T(8,128)(2,1)S(1)}, u32[]{:S(2)}, u32[]{:S(2)}) async-start(bf16[2,256,256]{2,1,0:T(8,128)(2,1)} %multiply_convert_fusion.3), calls=%async_computation.1 | async-start | bytes 524288 | tf_op jit(solution)/shard_map/all_to_all | solution.py:188
  153.2 10.2 %collective-permute-start.3 = (bf16[256,8,64]{0,2,1:T(8,128)(2,1)S(1)}, bf16[256,8,64]{0,2,1:T(8,128)(2,1)S(1)}, u32[]{:S(2)}, u32[]{:S(2)}) collective-permute-start(bf16[256,8,64]{0,2,1:T(8,128)(2,1)S(1)} %collective-permute-done.2), channel_id=1, source_target_pairs={{0,32},{8,40},{16,48},{24,56},{32,0},{40,8},{48,16},{56,24},{64,96... | collective-permute-start | bytes 786440 | tf_op jit(solution)/shard_map/ppermute | solution.py:48
  163.3 7.5 collective-permute-start.4
  270.6 10.6 %copy-start.2 = (f32[8,256,512]{2,1,0:T(8,128)}, f32[8,256,512]{2,1,0:T(8,128)S(1)}, u32[]{:S(2)}) copy-start(f32[8,256,512]{2,1,0:T(8,128)S(1)} %fusion.97) | copy-start | bytes 12582916
  311.4 19.1 %collective-permute-start.5 = (bf16[256,512]{0,1:T(8,128)(2,1)S(1)}, bf16[256,512]{0,1:T(8,128)(2,1)S(1)}, u32[]{:S(2)}, u32[]{:S(2)}) collective-permute-start(bf16[256,512]{0,1:T(8,128)(2,1)S(1)} %bitcast.254), channel_id=1, source_target_pairs={{0,8},{8,0},{16,24},{24,16},{32,40},{40,32},{48,56},{56,48},{64,72... | collective-permute-start | bytes 786440 | tf_op jit(solution)/shard_map/ppermute | solution.py:48
  330.5 37.8 %collective-permute-start.6 = (bf16[256,512]{0,1:T(8,128)(2,1)S(1)}, bf16[256,512]{0,1:T(8,128)(2,1)S(1)}, u32[]{:S(2)}, u32[]{:S(2)}) collective-permute-start(bf16[256,512]{0,1:T(8,128)(2,1)S(1)} %collective-permute-done.5), channel_id=1, source_target_pairs={{0,16},{8,24},{16,0},{24,8},{32,48},{40,56},{48,32},{56,40},{64,80... | collective-permute-start | bytes 786440 | tf_op jit(solution)/shard_map/ppermute | solution.py:48
  368.3 59.7 %collective-permute-start.7 = (bf16[256,512]{0,1:T(8,128)(2,1)S(1)}, bf16[256,512]{0,1:T(8,128)(2,1)S(1)}, u32[]{:S(2)}, u32[]{:S(2)}) collective-permute-start(bf16[256,512]{0,1:T(8,128)(2,1)S(1)} %collective-permute-done.6), channel_id=1, source_target_pairs={{0,32},{8,40},{16,48},{24,56},{32,0},{40,8},{48,16},{56,24},{64,96... | collective-permute-start | bytes 786440 | tf_op jit(solution)/shard_map/ppermute | solution.py:48
  428.1 310.9 %collective-permute-start.8 = (bf16[256,512]{0,1:T(8,128)(2,1)S(1)}, bf16[256,512]{0,1:T(8,128)(2,1)S(1)}, u32[]{:S(2)}, u32[]{:S(2)}) collective-permute-start(bf16[256,512]{0,1:T(8,128)(2,1)S(1)} %collective-permute-done.7), channel_id=1, source_target_pairs={{0,64},{8,72},{16,80},{24,88},{32,96},{40,104},{48,112},{56,120},{... | collective-permute-start | bytes 786440 | tf_op jit(solution)/shard_map/ppermute | solution.py:48
  738.9 7.9 %copy-start.8 = (f32[2,1,512]{2,1,0:T(1,128)S(1)}, f32[2,1,512]{2,1,0:T(1,128)}, u32[]{:S(2)}) copy-start(f32[2,1,512]{2,1,0:T(1,128)} %convert_element_type.154) | copy-start | bytes 12292
  746.9 3.8 copy-start.6
  747.1 6.8 copy-start.1
Sparse Core Ops, SparseCore 0:
  9.6 75.4 all-gather.8
  86.7 31.5 all-gather.16
  120.0 22.1 all-gather.10
  144.2 124.5 all-gather.14
  270.3 19.9 all-gather.18
  291.7 14.6 all-gather.12
where the time goes:
time: 772 us; the launch traced here: 761 us
  starting transfers between devices  224 us (29%)
  waiting for transfers between devices  201 us (26%)
  matrix products  178 us (23%)
  other arithmetic  68 us (9%)
  local copies, waits for them, and re-layouts  63.1 us (8%)
  between operations  14.4 us (2%)
  blocking collectives  11.4 us (1%)
    ppermute x8, starting transfers between devices, partner_2(): lax.ppermute(shard, axis, [(i, i ^ 1 << distance) for i in range(lax.axis...  210 us
    all_gather x1, waiting for transfers between devices, shards(): everything = lax.all_gather(key_value, 'sp', axis=1, tiled=True)  97.9 us
    dot_general x17, matrix products, stick_block(): jnp.einsum('htk,khd->thd', weight, value_heads, preferred_element_type=jn...  84 us
    dot_general x17, matrix products, stick_block(): jnp.einsum('thd,khd->htk', query, key_heads, preferred_element_type=jnp.f...  73.4 us
    another operation x52, other arithmetic  57.9 us
    all_gather x1, waiting for transfers between devices, in_one_piece(): whole, at, outs = (lax.all_gather(both, axis, axis=dim, tiled=True), 0, [])  57.7 us
    another operation x36, local copies, waits for them, and re-layouts  42.3 us
    all_gather x1, waiting for transfers between devices, shards(): lax.all_gather(w_out_attn, 'fs', axis=1, tiled=True)  17.3 us
  transfers between devices with their start and end apart: 17, of which 9 were waited for; matrix products, arithmetic and copies ran while one was open for 40% of the time, Pallas kernels for 0%

commit v1 on v0

--- a/solution.py
+++ b/solution.py
@@ -9,6 +9,19 @@
 POOL = 512
 POOL_GROUPS = 4
 EPS = 1e-06
+
+
+def find_domain(local_array):
+    n_peers_all = lax.psum(1, axis_name="sp")
+    s_next = local_array
+    log = [s_next]
+    work_now = [(c - 1, c) for c in range(1, n_peers_all)] + [(n_peers_all - 1, 0)]
+    for _ in [*range(n_peers_all - 1)]:
+        s_next = lax.ppermute(s_next, "sp", work_now)
+        log += [s_next]
+    taken_in = jnp.concatenate([*reversed(log)], 1)
+    out_arr = jnp.roll(taken_in, (lax.axis_index("sp") + 1) * s_next.shape[1], 1)
+    return out_arr
 
 
 def sent_to_all(shard, axis):
@@ -147,7 +160,7 @@
     score_scale = 1.0 / math.sqrt(HEAD_DIM)
     sp_count = lax.axis_size("sp")
     key_value = jnp.stack([key_heads, value_heads])
-    everything = lax.all_gather(key_value, "sp", axis=1, tiled=True)
+    everything = find_domain(key_value)
     half = row_count // 2
     bit_count = sp_count.bit_length() - 1
 

time: 772 us -> 1020 us (1.32)
  waiting for transfers between devices: 201 us -> 292 us
  starting transfers between devices: 224 us -> 305 us
  local copies, waits for them, and re-layouts: 63.1 us -> 115 us
  blocking collectives: 11.4 us -> 31 us
    ppermute x0 -> x15, waiting for transfers between devices: none -> 218 us  [find_domain(): s_next = lax.ppermute(s_next, 'sp', work_now)]
    all_gather x1 -> x0, waiting for transfers between devices: 97.9 us -> none  [shards(): everything = lax.all_gather(key_value, 'sp', axis=1, tiled=True)]
    ppermute x0 -> x15, starting transfers between devices: none -> 71.4 us  [find_domain(): s_next = lax.ppermute(s_next, 'sp', work_now)]
    unnamed x32 -> x88, local copies, waits for them, and re-layouts: 0.08 us -> 38.7 us
    all_to_all x1, starting transfers between devices: 6.59 us -> 24.1 us  [shards(): lax.all_to_all(pool_out, 'tp', split_axis=0, concat_axis=1, tiled=True)]
    all_gather x1, waiting for transfers between devices: 17.3 us -> 0.01 us  [shards(): lax.all_gather(w_out_attn, 'fs', axis=1, tiled=True)]
    all_gather x1, blocking collectives: 2.59 us -> 15.5 us  [shards(): lax.all_gather(pool_gain, 'tp', axis=0, tiled=True)]
  transfers between devices with their start and end apart: 17 -> 31, of which waited for: 9 -> 19; matrix products, arithmetic and copies ran while one was open for 40% -> 34% of each run, Pallas kernels for 0% -> 0%
where the time goes in v1:
time: 1020 us; the launch traced here: 1010 us
  starting transfers between devices  305 us (30%)
  waiting for transfers between devices  292 us (29%)
  matrix products  181 us (18%)
  local copies, waits for them, and re-layouts  115 us (11%)
  other arithmetic  72.1 us (7%)
  blocking collectives  31 us (3%)
  between operations  14.3 us (1%)
    ppermute x15, waiting for transfers between devices, find_domain(): s_next = lax.ppermute(s_next, 'sp', work_now)  218 us
    ppermute x8, starting transfers between devices, partner_2(): lax.ppermute(shard, axis, [(i, i ^ 1 << distance) for i in range(lax.axis...  203 us
    dot_general x17, matrix products, stick_block(): jnp.einsum('htk,khd->thd', weight, value_heads, preferred_element_type=jn...  84.5 us
    dot_general x17, matrix products, stick_block(): jnp.einsum('thd,khd->htk', query, key_heads, preferred_element_type=jnp.f...  75.7 us
    ppermute x15, starting transfers between devices, find_domain(): s_next = lax.ppermute(s_next, 'sp', work_now)  71.4 us
    all_gather x1, waiting for transfers between devices, in_one_piece(): whole, at, outs = (lax.all_gather(both, axis, axis=dim, tiled=True), 0, [])  58.5 us
    another operation x52, other arithmetic  57.8 us
    another operation x36, local copies, waits for them, and re-layouts  41.8 us
  transfers between devices with their start and end apart: 31, of which 19 were waited for; matrix products, arithmetic and copies ran while one was open for 34% of the time, Pallas kernels for 0%

profile of v1, /device:TPU:103, one launch (start us, length us, event | category | flops | bytes accessed | tf_op | source)
XLA Modules:
  0.0 1013.1 jit_solution(9693493390536112752)
XLA Ops:
  11.1 5.5 all-to-all-start
  26.6 58.5 %all-gather.8.cloned.1.call-done = bf16[2048,1792]{1,0:T(8,128)(2,1)} async-done(((bf16[512,1792]{1,0:T(8,128)(2,1)}), bf16[2048,1792]{1,0:T(8,128)(2,1)}) %all-gather.8.cloned.1.call-update) | async-done | bytes 7340048 | tf_op jit(solution)/shard_map/all_gather | solution.py:47
  99.9 23.9 %collective-permute-done.1 = bf16[2,512,8,64]{1,3,2,0:T(8,128)(2,1)S(1)} collective-permute-done((bf16[2,512,8,64]{1,3,2,0:T(8,128)(2,1)S(1)}, bf16[2,512,8,64]{1,3,2,0:T(8,128)(2,1)S(1)}, u32[]{:S(2)}, u32[]{:S(2)}) %collective-permute-start.1) | collective-permute-done | bytes 1048608 | tf_op jit(solution)/shard_map/ppermute | solution.py:20
  128.1 20.8 %collective-permute-done.2 = bf16[2,512,8,64]{1,3,2,0:T(8,128)(2,1)S(1)} collective-permute-done((bf16[2,512,8,64]{1,3,2,0:T(8,128)(2,1)S(1)}, bf16[2,512,8,64]{1,3,2,0:T(8,128)(2,1)S(1)}, u32[]{:S(2)}, u32[]{:S(2)}) %collective-permute-start.2) | collective-permute-done | bytes 1048608 | tf_op jit(solution)/shard_map/ppermute | solution.py:20
  149.9 5.5 collective-permute-start.3
  155.4 20.0 %collective-permute-done.3 = bf16[2,512,8,64]{1,3,2,0:T(8,128)(2,1)} collective-permute-done((bf16[2,512,8,64]{1,3,2,0:T(8,128)(2,1)S(1)}, bf16[2,512,8,64]{1,3,2,0:T(8,128)(2,1)}, u32[]{:S(2)}, u32[]{:S(2)}) %collective-permute-start.3) | collective-permute-done | bytes 1048608 | tf_op jit(solution)/shard_map/ppermute | solution.py:20
  175.4 5.6 collective-permute-start.4
  181.1 19.4 %collective-permute-done.4 = bf16[2,512,8,64]{1,3,2,0:T(8,128)(2,1)} collective-permute-done((bf16[2,512,8,64]{1,3,2,0:T(8,128)(2,1)}, bf16[2,512,8,64]{1,3,2,0:T(8,128)(2,1)}, u32[]{:S(2)}, u32[]{:S(2)}) %collective-permute-start.4) | collective-permute-done | bytes 1048608 | tf_op jit(solution)/shard_map/ppermute | solution.py:20
  200.5 5.5 collective-permute-start.5
  206.0 18.6 %collective-permute-done.5 = bf16[2,512,8,64]{1,3,2,0:T(8,128)(2,1)S(1)} collective-permute-done((bf16[2,512,8,64]{1,3,2,0:T(8,128)(2,1)}, bf16[2,512,8,64]{1,3,2,0:T(8,128)(2,1)S(1)}, u32[]{:S(2)}, u32[]{:S(2)}) %collective-permute-start.5) | collective-permute-done | bytes 1048608 | tf_op jit(solution)/shard_map/ppermute | solution.py:20
  231.0 17.4 %collective-permute-done.6 = bf16[2,512,8,64]{1,3,2,0:T(8,128)(2,1)} collective-permute-done((bf16[2,512,8,64]{1,3,2,0:T(8,128)(2,1)S(1)}, bf16[2,512,8,64]{1,3,2,0:T(8,128)(2,1)}, u32[]{:S(2)}, u32[]{:S(2)}) %collective-permute-start.6) | collective-permute-done | bytes 1048608 | tf_op jit(solution)/shard_map/ppermute | solution.py:20
  248.4 5.6 collective-permute-start.7
  254.1 16.8 %collective-permute-done.7 = bf16[2,512,8,64]{1,3,2,0:T(8,128)(2,1)} collective-permute-done((bf16[2,512,8,64]{1,3,2,0:T(8,128)(2,1)}, bf16[2,512,8,64]{1,3,2,0:T(8,128)(2,1)}, u32[]{:S(2)}, u32[]{:S(2)}) %collective-permute-start.7) | collective-permute-done | bytes 1048608 | tf_op jit(solution)/shard_map/ppermute | solution.py:20
  276.4 16.1 %collective-permute-done.8 = bf16[2,512,8,64]{1,3,2,0:T(8,128)(2,1)} collective-permute-done((bf16[2,512,8,64]{1,3,2,0:T(8,128)(2,1)}, bf16[2,512,8,64]{1,3,2,0:T(8,128)(2,1)}, u32[]{:S(2)}, u32[]{:S(2)}) %collective-permute-start.8) | collective-permute-done | bytes 1048608 | tf_op jit(solution)/shard_map/ppermute | solution.py:20
  298.1 16.0 %collective-permute-done.9 = bf16[2,512,8,64]{1,3,2,0:T(8,128)(2,1)} collective-permute-done((bf16[2,512,8,64]{1,3,2,0:T(8,128)(2,1)}, bf16[2,512,8,64]{1,3,2,0:T(8,128)(2,1)}, u32[]{:S(2)}, u32[]{:S(2)}) %collective-permute-start.9) | collective-permute-done | bytes 1048608 | tf_op jit(solution)/shard_map/ppermute | solution.py:20
  319.6 16.1 %collective-permute-done.10 = bf16[2,512,8,64]{1,3,2,0:T(8,128)(2,1)} collective-permute-done((bf16[2,512,8,64]{1,3,2,0:T(8,128)(2,1)}, bf16[2,512,8,64]{1,3,2,0:T(8,128)(2,1)}, u32[]{:S(2)}, u32[]{:S(2)}) %collective-permute-start.10) | collective-permute-done | bytes 1048608 | tf_op jit(solution)/shard_map/ppermute | solution.py:20
  341.2 16.1 %collective-permute-done.11 = bf16[2,512,8,64]{1,3,2,0:T(8,128)(2,1)} collective-permute-done((bf16[2,512,8,64]{1,3,2,0:T(8,128)(2,1)}, bf16[2,512,8,64]{1,3,2,0:T(8,128)(2,1)}, u32[]{:S(2)}, u32[]{:S(2)}) %collective-permute-start.11) | collective-permute-done | bytes 1048608 | tf_op jit(solution)/shard_map/ppermute | solution.py:20
  362.9 15.5 %all-gather = bf16[2,1,256]{2,1,0:T(2,128)(2,1)S(1)} all-gather(bf16[1,1,256]{2,1,0:T(2,128)(2,1)S(1)} %reshape.262), channel_id=1, replica_groups=mesh['sp'=16,'fs'=4,'tp'=2] {'tp'}, dimensions={0}, use_global_device_ids=true | all-gather | bytes 1536 | tf_op jit(solution)/shard_map/all_gather | solution.py:207
  395.2 5.7 collective-permute-done.13
  412.2 11.5 %collective-permute-done.14 = bf16[2,512,8,64]{1,3,2,0:T(8,128)(2,1)S(1)} collective-permute-done((bf16[2,512,8,64]{1,3,2,0:T(8,128)(2,1)}, bf16[2,512,8,64]{1,3,2,0:T(8,128)(2,1)S(1)}, u32[]{:S(2)}, u32[]{:S(2)}) %collective-permute-start.14) | collective-permute-done | bytes 1048608 | tf_op jit(solution)/shard_map/ppermute | solution.py:20
  430.6 24.1 %all-to-all-start.1 = ((bf16[2,256,256]{2,1,0:T(8,128)(2,1)}), bf16[2,256,256]{2,1,0:T(8,128)(2,1)S(1)}, u32[]{:S(2)}, u32[]{:S(2)}) async-start(bf16[2,256,256]{2,1,0:T(8,128)(2,1)} %multiply_convert_fusion.3), calls=%async_computation.1 | async-start | bytes 524288 | tf_op jit(solution)/shard_map/all_to_all | solution.py:201
  456.8 7.4 collective-permute-done.17
  503.4 8.9 constant_dynamic-slice_fusion
  520.9 10.8 %fusion.63 = (f32[8,256,512]{2,1,0:T(8,128)}, f32[8,256,512]{2,1,0:T(8,128)}, f32[8,256,512]{2,1,0:T(8,128)}) fusion(f32[8]{0:T(128)S(1)} %copy-done.24, pred[256,512]{1,0:T(8,128)(4,1)S(1)} %copy-done.15, f32[8,256,512]{2,1,0:T(8,128)} %fusion.97, pred[256,512]{1,0:T(8,128)(4,1)S(1)} %copy-done.16, ...), kind=kOutput, calls=%fused_computation.79 | convolution fusion | flops 155189248 | bytes 17826308 | tf_op jit(solution)/shard_map/thd,khd->htk/dot_general | solution.py:72
  554.7 6.7 fusion.88
  561.6 9.7 collective-permute-start.20
  575.0 30.0 %collective-permute-start.21 = (bf16[256,512]{0,1:T(8,128)(2,1)S(1)}, bf16[256,512]{0,1:T(8,128)(2,1)S(1)}, u32[]{:S(2)}, u32[]{:S(2)}) collective-permute-start(bf16[256,512]{0,1:T(8,128)(2,1)S(1)} %collective-permute-done.20), channel_id=1, source_target_pairs={{0,16},{8,24},{16,0},{24,8},{32,48},{40,56},{48,32},{56,40},{64,80... | collective-permute-start | bytes 786440 | tf_op jit(solution)/shard_map/ppermute | solution.py:61
  614.5 55.0 %collective-permute-start.22 = (bf16[256,512]{0,1:T(8,128)(2,1)S(1)}, bf16[256,512]{0,1:T(8,128)(2,1)S(1)}, u32[]{:S(2)}, u32[]{:S(2)}) collective-permute-start(bf16[256,512]{0,1:T(8,128)(2,1)S(1)} %collective-permute-done.21), channel_id=1, source_target_pairs={{0,32},{8,40},{16,48},{24,56},{32,0},{40,8},{48,16},{56,24},{64,96... | collective-permute-start | bytes 786440 | tf_op jit(solution)/shard_map/ppermute | solution.py:61
  669.5 6.6 fusion.85
  676.2 107.7 %collective-permute-start.23 = (bf16[256,512]{0,1:T(8,128)(2,1)S(1)}, bf16[256,512]{0,1:T(8,128)(2,1)S(1)}, u32[]{:S(2)}, u32[]{:S(2)}) collective-permute-start(bf16[256,512]{0,1:T(8,128)(2,1)S(1)} %collective-permute-done.22), channel_id=1, source_target_pairs={{0,64},{8,72},{16,80},{24,88},{32,96},{40,104},{48,112},{56,120},{... | collective-permute-start | bytes 786440 | tf_op jit(solution)/shard_map/ppermute | solution.py:61
  783.9 200.5 %while.24 = (s32[]{:T(128)}, f32[256,8,64]{0,2,1:T(8,128)S(1)}, f32[8,256]{1,0:T(8,128)S(1)}, s32[]{:T(128)}, s32[]{:T(128)}, /*index=5*/bf16[2,8192,8,64]{1,3,2...) while((s32[]{:T(128)}, f32[256,8,64]{0,2,1:T(8,128)S(1)}, ...), condition=%wide.region_9.10_spmd, body=%wide.region_6.9_spmd.sunk | while | flops 426934272 | bytes 44548372 | solution.py:184
  984.7 13.7 %all_to_all.28 = bf16[2,256,512]{2,1,0:T(8,128)(2,1)S(1)} all-to-all(bf16[2,256,512]{2,1,0:T(8,128)(2,1)S(1)} %bitcast.251), channel_id=1, replica_groups=mesh['sp'=16,'fs'=4,'tp'=2] {'tp'}, dimensions={0} | all-to-all | bytes 1048576 | tf_op jit(solution)/shard_map/all_to_all | solution.py:202
  (356 shorter events, 396.5 us)
Async XLA Ops:
  6.5 400.7 %copy-start = (bf16[2,128,128]{2,1,0:T(8,128)(2,1)S(1)}, bf16[2,128,128]{2,1,0:T(8,128)(2,1)}, u32[]{:S(2)}) copy-start(bf16[2,128,128]{2,1,0:T(8,128)(2,1)} %param.28) | copy-start | bytes 196612
  6.5 78.6 %all-gather.8.cloned.1.call-start = ((), (), s32[]{:S(2)}) async-start(), calls=%async_computation.3 | async-start | bytes 9175040 | tf_op jit(solution)/shard_map/all_gather | solution.py:47
  11.1 8.2 all-to-all-start
  16.7 281.4 %all-gather.14.cloned.1.call-start = ((), (), s32[]{:S(2)}) async-start(), calls=%async_computation.6 | async-start | bytes 2621440 | tf_op jit(solution)/shard_map/all_gather | solution.py:198
  99.9 23.9 %collective-permute-start.1 = (bf16[2,512,8,64]{1,3,2,0:T(8,128)(2,1)S(1)}, bf16[2,512,8,64]{1,3,2,0:T(8,128)(2,1)S(1)}, u32[]{:S(2)}, u32[]{:S(2)}) collective-permute-start(bf16[2,512,8,64]{1,3,2,0:T(8,128)(2,1)S(1)} %pad_maximum_fusion.1), channel_id=1, source_target_pairs={{0,8},{8,16},{16,24},{24,32},{32,40},{40,48},{48,56},{56,64},{64,7... | collective-permute-start | bytes 3145736 | tf_op jit(solution)/shard_map/ppermute | solution.py:20
  124.8 24.2 %collective-permute-start.2 = (bf16[2,512,8,64]{1,3,2,0:T(8,128)(2,1)S(1)}, bf16[2,512,8,64]{1,3,2,0:T(8,128)(2,1)S(1)}, u32[]{:S(2)}, u32[]{:S(2)}) collective-permute-start(bf16[2,512,8,64]{1,3,2,0:T(8,128)(2,1)S(1)} %collective-permute-done.1), channel_id=1, source_target_pairs={{0,8},{8,16},{16,24},{24,32},{32,40},{40,48},{48,56},{56,64},{64,7... | collective-permute-start | bytes 3145736 | tf_op jit(solution)/shard_map/ppermute | solution.py:20
  149.9 25.5 %collective-permute-start.3 = (bf16[2,512,8,64]{1,3,2,0:T(8,128)(2,1)S(1)}, bf16[2,512,8,64]{1,3,2,0:T(8,128)(2,1)}, u32[]{:S(2)}, u32[]{:S(2)}) collective-permute-start(bf16[2,512,8,64]{1,3,2,0:T(8,128)(2,1)S(1)} %collective-permute-done.2), channel_id=1, source_target_pairs={{0,8},{8,16},{16,24},{24,32},{32,40},{40,48},{48,56},{56,64},{64,7... | collective-permute-start | bytes 3145736 | tf_op jit(solution)/shard_map/ppermute | solution.py:20
  175.4 25.1 %collective-permute-start.4 = (bf16[2,512,8,64]{1,3,2,0:T(8,128)(2,1)}, bf16[2,512,8,64]{1,3,2,0:T(8,128)(2,1)}, u32[]{:S(2)}, u32[]{:S(2)}) collective-permute-start(bf16[2,512,8,64]{1,3,2,0:T(8,128)(2,1)} %collective-permute-done.3), channel_id=1, source_target_pairs={{0,8},{8,16},{16,24},{24,32},{32,40},{40,48},{48,56},{56,64},{64,7... | collective-permute-start | bytes 3145736 | tf_op jit(solution)/shard_map/ppermute | solution.py:20
  181.1 204.1 %all-gather.10.cloned.1.call-start = ((), (), s32[]{:S(2)}) async-start(), calls=%async_computation.4 | async-start | bytes 1310720 | tf_op jit(solution)/shard_map/all_gather | solution.py:197
  200.5 24.1 %collective-permute-start.5 = (bf16[2,512,8,64]{1,3,2,0:T(8,128)(2,1)}, bf16[2,512,8,64]{1,3,2,0:T(8,128)(2,1)S(1)}, u32[]{:S(2)}, u32[]{:S(2)}) collective-permute-start(bf16[2,512,8,64]{1,3,2,0:T(8,128)(2,1)} %collective-permute-done.4), channel_id=1, source_target_pairs={{0,8},{8,16},{16,24},{24,32},{32,40},{40,48},{48,56},{56,64},{64,7... | collective-permute-start | bytes 3145736 | tf_op jit(solution)/shard_map/ppermute | solution.py:20
  225.6 22.8 %collective-permute-start.6 = (bf16[2,512,8,64]{1,3,2,0:T(8,128)(2,1)S(1)}, bf16[2,512,8,64]{1,3,2,0:T(8,128)(2,1)}, u32[]{:S(2)}, u32[]{:S(2)}) collective-permute-start(bf16[2,512,8,64]{1,3,2,0:T(8,128)(2,1)S(1)} %collective-permute-done.5), channel_id=1, source_target_pairs={{0,8},{8,16},{16,24},{24,32},{32,40},{40,48},{48,56},{56,64},{64,7... | collective-permute-start | bytes 3145736 | tf_op jit(solution)/shard_map/ppermute | solution.py:20
  248.4 22.5 %collective-permute-start.7 = (bf16[2,512,8,64]{1,3,2,0:T(8,128)(2,1)}, bf16[2,512,8,64]{1,3,2,0:T(8,128)(2,1)}, u32[]{:S(2)}, u32[]{:S(2)}) collective-permute-start(bf16[2,512,8,64]{1,3,2,0:T(8,128)(2,1)} %collective-permute-done.6), channel_id=1, source_target_pairs={{0,8},{8,16},{16,24},{24,32},{32,40},{40,48},{48,56},{56,64},{64,7... | collective-permute-start | bytes 3145736 | tf_op jit(solution)/shard_map/ppermute | solution.py:20
  254.0 745.3 %all-gather.16.cloned.1.call-start = ((), (), s32[]{:S(2)}) async-start(), calls=%async_computation.7 | async-start | bytes 6291456 | tf_op jit(solution)/shard_map/all_gather | solution.py:206
  270.9 21.6 %collective-permute-start.8 = (bf16[2,512,8,64]{1,3,2,0:T(8,128)(2,1)}, bf16[2,512,8,64]{1,3,2,0:T(8,128)(2,1)}, u32[]{:S(2)}, u32[]{:S(2)}) collective-permute-start(bf16[2,512,8,64]{1,3,2,0:T(8,128)(2,1)} %collective-permute-done.7), channel_id=1, source_target_pairs={{0,8},{8,16},{16,24},{24,32},{32,40},{40,48},{48,56},{56,64},{64,7... | collective-permute-start | bytes 3145736 | tf_op jit(solution)/shard_map/ppermute | solution.py:20
  292.5 21.6 %collective-permute-start.9 = (bf16[2,512,8,64]{1,3,2,0:T(8,128)(2,1)}, bf16[2,512,8,64]{1,3,2,0:T(8,128)(2,1)}, u32[]{:S(2)}, u32[]{:S(2)}) collective-permute-start(bf16[2,512,8,64]{1,3,2,0:T(8,128)(2,1)} %collective-permute-done.8), channel_id=1, source_target_pairs={{0,8},{8,16},{16,24},{24,32},{32,40},{40,48},{48,56},{56,64},{64,7... | collective-permute-start | bytes 3145736 | tf_op jit(solution)/shard_map/ppermute | solution.py:20
  298.0 704.9 %all-gather.12.cloned.1.call-start = ((), (), s32[]{:S(2)}) async-start(), calls=%async_computation.5 | async-start | bytes 3145728 | tf_op jit(solution)/shard_map/all_gather | solution.py:205
  314.1 21.6 %collective-permute-start.10 = (bf16[2,512,8,64]{1,3,2,0:T(8,128)(2,1)}, bf16[2,512,8,64]{1,3,2,0:T(8,128)(2,1)}, u32[]{:S(2)}, u32[]{:S(2)}) collective-permute-start(bf16[2,512,8,64]{1,3,2,0:T(8,128)(2,1)} %collective-permute-done.9), channel_id=1, source_target_pairs={{0,8},{8,16},{16,24},{24,32},{32,40},{40,48},{48,56},{56,64},{64,7... | collective-permute-start | bytes 3145736 | tf_op jit(solution)/shard_map/ppermute | solution.py:20
  335.7 21.6 %collective-permute-start.11 = (bf16[2,512,8,64]{1,3,2,0:T(8,128)(2,1)}, bf16[2,512,8,64]{1,3,2,0:T(8,128)(2,1)}, u32[]{:S(2)}, u32[]{:S(2)}) collective-permute-start(bf16[2,512,8,64]{1,3,2,0:T(8,128)(2,1)} %collective-permute-done.10), channel_id=1, source_target_pairs={{0,8},{8,16},{16,24},{24,32},{32,40},{40,48},{48,56},{56,64},{64,7... | collective-permute-start | bytes 3145736 | tf_op jit(solution)/shard_map/ppermute | solution.py:20
  357.3 25.0 %collective-permute-start.12 = (bf16[2,512,8,64]{1,3,2,0:T(8,128)(2,1)}, bf16[2,512,8,64]{1,3,2,0:T(8,128)(2,1)}, u32[]{:S(2)}, u32[]{:S(2)}) collective-permute-start(bf16[2,512,8,64]{1,3,2,0:T(8,128)(2,1)} %collective-permute-done.11), channel_id=1, source_target_pairs={{0,8},{8,16},{16,24},{24,32},{32,40},{40,48},{48,56},{56,64},{64,7... | collective-permute-start | bytes 3145736 | tf_op jit(solution)/shard_map/ppermute | solution.py:20
  382.3 18.6 %collective-permute-start.13 = (bf16[2,512,8,64]{1,3,2,0:T(8,128)(2,1)}, bf16[2,512,8,64]{1,3,2,0:T(8,128)(2,1)}, u32[]{:S(2)}, u32[]{:S(2)}) collective-permute-start(bf16[2,512,8,64]{1,3,2,0:T(8,128)(2,1)} %collective-permute-done.12), channel_id=1, source_target_pairs={{0,8},{8,16},{16,24},{24,32},{32,40},{40,48},{48,56},{56,64},{64,7... | collective-permute-start | bytes 3145736 | tf_op jit(solution)/shard_map/ppermute | solution.py:20
  387.9 19.3 %collective-permute-start = (bf16[16,256]{1,0:T(8,128)(2,1)S(1)}, bf16[16,256]{1,0:T(8,128)(2,1)S(1)}, u32[]{:S(2)}, u32[]{:S(2)}) collective-permute-start(bf16[16,256]{1,0:T(8,128)(2,1)S(1)} %slice.170), channel_id=1, source_target_pairs={{0,8},{8,16},{16,24},{24,32},{32,40},{40,48},{48,56},{56,64},{64,7... | collective-permute-start | bytes 24584 | tf_op jit(solution)/shard_map/ppermute | solution.py:57
  400.9 22.8 %collective-permute-start.14 = (bf16[2,512,8,64]{1,3,2,0:T(8,128)(2,1)}, bf16[2,512,8,64]{1,3,2,0:T(8,128)(2,1)S(1)}, u32[]{:S(2)}, u32[]{:S(2)}) collective-permute-start(bf16[2,512,8,64]{1,3,2,0:T(8,128)(2,1)} %collective-permute-done.13), channel_id=1, source_target_pairs={{0,8},{8,16},{16,24},{24,32},{32,40},{40,48},{48,56},{56,64},{64,7... | collective-permute-start | bytes 3145736 | tf_op jit(solution)/shard_map/ppermute | solution.py:20
  407.2 47.5 %collective-permute-start.16 = (bf16[256,8,64]{0,2,1:T(8,128)(2,1)}, bf16[256,8,64]{0,2,1:T(8,128)(2,1)}, u32[]{:S(2)}, u32[]{:S(2)}) collective-permute-start(bf16[256,8,64]{0,2,1:T(8,128)(2,1)} %get-tuple-element.132), channel_id=1, source_target_pairs={{0,8},{8,0},{16,24},{24,16},{32,40},{40,32},{48,56},{56,48},{64,72... | collective-permute-start | bytes 786440 | tf_op jit(solution)/shard_map/ppermute | solution.py:61
  423.7 48.1 %collective-permute-start.15 = (bf16[2,512,8,64]{1,3,2,0:T(8,128)(2,1)S(1)}, bf16[2,512,8,64]{1,3,2,0:T(8,128)(2,1)}, u32[]{:S(2)}, u32[]{:S(2)}) collective-permute-start(bf16[2,512,8,64]{1,3,2,0:T(8,128)(2,1)S(1)} %collective-permute-done.14), channel_id=1, source_target_pairs={{0,8},{8,16},{16,24},{24,32},{32,40},{40,48},{48,56},{56,64},{64,7... | collective-permute-start | bytes 3145736 | tf_op jit(solution)/shard_map/ppermute | solution.py:20
  430.6 25.3 %all-to-all-start.1 = ((bf16[2,256,256]{2,1,0:T(8,128)(2,1)}), bf16[2,256,256]{2,1,0:T(8,128)(2,1)S(1)}, u32[]{:S(2)}, u32[]{:S(2)}) async-start(bf16[2,256,256]{2,1,0:T(8,128)(2,1)} %multiply_convert_fusion.3), calls=%async_computation.1 | async-start | bytes 524288 | tf_op jit(solution)/shard_map/all_to_all | solution.py:201
  454.6 9.6 collective-permute-start.17
  464.2 7.1 collective-permute-start.18
  471.3 40.9 %collective-permute-start.19 = (bf16[256,8,64]{0,2,1:T(8,128)(2,1)S(1)}, bf16[256,8,64]{0,2,1:T(8,128)(2,1)S(1)}, u32[]{:S(2)}, u32[]{:S(2)}) collective-permute-start(bf16[256,8,64]{0,2,1:T(8,128)(2,1)S(1)} %collective-permute-done.18), channel_id=1, source_target_pairs={{0,64},{8,72},{16,80},{24,88},{32,96},{40,104},{48,112},{56,120},{... | collective-permute-start | bytes 786440 | tf_op jit(solution)/shard_map/ppermute | solution.py:61
  561.6 13.5 %collective-permute-start.20 = (bf16[256,512]{0,1:T(8,128)(2,1)S(1)}, bf16[256,512]{0,1:T(8,128)(2,1)S(1)}, u32[]{:S(2)}, u32[]{:S(2)}) collective-permute-start(bf16[256,512]{0,1:T(8,128)(2,1)S(1)} %bitcast.256), channel_id=1, source_target_pairs={{0,8},{8,0},{16,24},{24,16},{32,40},{40,32},{48,56},{56,48},{64,72... | collective-permute-start | bytes 786440 | tf_op jit(solution)/shard_map/ppermute | solution.py:61
  575.0 39.4 %collective-permute-start.21 = (bf16[256,512]{0,1:T(8,128)(2,1)S(1)}, bf16[256,512]{0,1:T(8,128)(2,1)S(1)}, u32[]{:S(2)}, u32[]{:S(2)}) collective-permute-start(bf16[256,512]{0,1:T(8,128)(2,1)S(1)} %collective-permute-done.20), channel_id=1, source_target_pairs={{0,16},{8,24},{16,0},{24,8},{32,48},{40,56},{48,32},{56,40},{64,80... | collective-permute-start | bytes 786440 | tf_op jit(solution)/shard_map/ppermute | solution.py:61
  614.5 61.7 %collective-permute-start.22 = (bf16[256,512]{0,1:T(8,128)(2,1)S(1)}, bf16[256,512]{0,1:T(8,128)(2,1)S(1)}, u32[]{:S(2)}, u32[]{:S(2)}) collective-permute-start(bf16[256,512]{0,1:T(8,128)(2,1)S(1)} %collective-permute-done.21), channel_id=1, source_target_pairs={{0,32},{8,40},{16,48},{24,56},{32,0},{40,8},{48,16},{56,24},{64,96... | collective-permute-start | bytes 786440 | tf_op jit(solution)/shard_map/ppermute | solution.py:61
  676.2 308.3 %collective-permute-start.23 = (bf16[256,512]{0,1:T(8,128)(2,1)S(1)}, bf16[256,512]{0,1:T(8,128)(2,1)S(1)}, u32[]{:S(2)}, u32[]{:S(2)}) collective-permute-start(bf16[256,512]{0,1:T(8,128)(2,1)S(1)} %collective-permute-done.22), channel_id=1, source_target_pairs={{0,64},{8,72},{16,80},{24,88},{32,96},{40,104},{48,112},{56,120},{... | collective-permute-start | bytes 786440 | tf_op jit(solution)/shard_map/ppermute | solution.py:61
  (27 other events, 892.8 us)
Sparse Core Ops, SparseCore 0:
  9.6 75.4 all-gather.7
  181.2 33.9 all-gather.13
  254.1 27.9 all-gather.9
  298.2 25.5 all-gather.15
  385.4 29.1 all-gather.11
